TPU v7x, 32 devices: a whole 2x2x4 slice. The times are simulated.
32 devices in a mesh: fs: 4 (over y, x), tp: 8 (over z, core).
Axes of the slice: x: 2, y: 2, z: 4, core: 2. Of those that a mesh axis runs over, the one named last changes fastest.
Arguments:
- stream_in: bfloat16 [4096, 4096], P(('fs', 'tp')), may hold values from -6 to 6
- mixer_out: bfloat16 [4096, 4096], P(('fs', 'tp')), may hold values from -6 to 6
- mix_gain: float32 [4096], replicated, may hold values from 0.1 to 1.9
- pre_gain: float32 [4096], replicated, may hold values from 0.1 to 1.9
- gate_weight: float32 [4096, 6144], P('fs', 'tp'), may hold values from -0.09375 to 0.09375
- up_weight: float32 [4096, 6144], P('fs', 'tp'), may hold values from -0.09375 to 0.09375
- gate_scale: float32 [6144], P('tp'), may hold values from 0.5 to 2
- up_scale: float32 [6144], P('tp'), may hold values from 0.5 to 2
Outputs:
- hidden: bfloat16 [4096, 6144], P('fs', 'tp')
- stream: bfloat16 [4096, 4096], P(('fs', 'tp'))
All inputs are finite; a program needn't handle non-finite values.
Results may differ from a plain program's by a relative error of at most 0.0082.
Values may be sent and summed in bfloat16 or wider, within the bound.
A program may use at most 128 MiB of HBM per device.

v0:
```python
import jax
import jax.numpy as jnp
from jax import lax
from jax.sharding import PartitionSpec as P

epsilon = 1e-06


def rms_scaled(values, gain):
    return values * lax.rsqrt(jnp.mean(values * values, axis=-1, keepdims=True) + epsilon) * gain


def on_device(
    stream_in, mixer_out, mix_gain, pre_gain, gate_weight, up_weight, gate_scale, up_scale
):
    mixed = stream_in.astype(jnp.float32) + rms_scaled(mixer_out.astype(jnp.float32), mix_gain)
    stream = mixed.astype(jnp.bfloat16)
    normed = rms_scaled(stream.astype(jnp.float32), pre_gain).astype(jnp.bfloat16)
    gate_cast = gate_weight.astype(jnp.bfloat16)
    up_cast = up_weight.astype(jnp.bfloat16)
    gate_full, up_full = (
        lax.all_gather(gate_cast, "fs", axis=0, tiled=True),
        lax.all_gather(up_cast, "fs", axis=0, tiled=True),
    )
    piece = lax.all_gather(normed, "tp", axis=0, tiled=True)
    gate = jnp.dot(piece, gate_full, preferred_element_type=jnp.float32) * gate_scale
    up = jnp.dot(piece, up_full, preferred_element_type=jnp.float32) * up_scale
    hidden = (jax.nn.silu(gate) * up).astype(jnp.bfloat16)
    return (hidden, stream)


def solution(mesh):
    return jax.shard_map(
        on_device,
        mesh=mesh,
        in_specs=(
            P(("fs", "tp"), None),
            P(("fs", "tp"), None),
            P(),
            P(),
            P("fs", "tp"),
            P("fs", "tp"),
            P("tp"),
            P("tp"),
        ),
        out_specs=(P("fs", "tp"), P(("fs", "tp"), None)),
        check_vma=False,
    )
```

profile of v0, /device:TPU:0, one launch (start us, length us, event | category | flops | bytes accessed | tf_op | source)
XLA Modules:
  0.0 256.1 jit_solution(6884719773406794379)
XLA Ops:
  7.2 0.0 copy-start.1
  7.2 0.0 copy-start.3
  7.2 0.0 copy-start.2
  7.2 0.0 all-gather.6.cloned.1.call-start
  7.2 3.3 %convert_element_type.29 = bf16[1024,768]{1,0:T(8,128)(2,1)} convert(f32[1024,768]{1,0:T(8,128)} %param.12) | non-fusion elementwise | flops 786432 | bytes 4718592 | tf_op jit(solution)/shard_map/convert_element_type | solution.py:19
  10.6 0.0 copy-start.4
  10.6 0.0 all-gather.6.cloned.1.call-update
  10.6 0.0 all-gather.4.cloned.1.call-start
  10.6 0.0 copy-done.1
  10.6 0.3 fusion
  10.9 0.0 copy-done.3
  11.0 0.0 copy-done.2
  11.0 0.7 fusion.4
  11.7 0.0 copy-start
  11.7 0.0 copy-done.4
  11.7 1.3 fusion.6
  13.1 0.0 all-gather.4.cloned.1.call-update
  13.1 0.0 all-gather.8.cloned.1.call-start
  13.2 3.2 %convert_element_type.30 = bf16[1024,768]{1,0:T(8,128)(2,1)} convert(f32[1024,768]{1,0:T(8,128)} %param.13) | non-fusion elementwise | flops 786432 | bytes 4718592 | tf_op jit(solution)/shard_map/convert_element_type | solution.py:20
  16.4 0.0 copy-done
  16.4 0.0 all-gather.8.cloned.1.call-update
  16.4 0.0 copy-start.5
  16.4 0.0 copy-start.6
  16.4 67.1 %all-gather.6.cloned.1.call-done = bf16[4096,768]{1,0:T(8,128)(2,1)} async-done(((bf16[1024,768]{1,0:T(8,128)(2,1)}), bf16[4096,768]{1,0:T(8,128)(2,1)}) %all-gather.6.cloned.1.call-update) | async-done | bytes 6291472 | tf_op jit(solution)/shard_map/all_gather | solution.py:22
  83.5 83.7 %all-gather.4.cloned.1.call-done = bf16[1024,4096]{1,0:T(8,128)(2,1)} async-done(((bf16[128,4096]{1,0:T(8,128)(2,1)}), bf16[1024,4096]{1,0:T(8,128)(2,1)}) %all-gather.4.cloned.1.call-update) | async-done | bytes 8388624 | tf_op jit(solution)/shard_map/all_gather | solution.py:25
  167.2 10.9 %fusion.8 = f32[1024,768]{1,0:T(8,128)S(1)} fusion(bf16[1024,4096]{1,0:T(8,128)(2,1)} %all-gather.4.cloned.1.call-done, bf16[4096,768]{1,0:T(8,128)(2,1)} %all-gather.6.cloned.1.call-done), kind=kOutput, calls=%fused_computation.14 | convolution fusion | flops 6442450944 | bytes 17825792 | tf_op jit(solution)/shard_map/dot_general | solution.py:26
  178.1 59.5 %all-gather.8.cloned.1.call-done = bf16[4096,768]{1,0:T(8,128)(2,1)} async-done(((bf16[1024,768]{1,0:T(8,128)(2,1)}), bf16[4096,768]{1,0:T(8,128)(2,1)}) %all-gather.8.cloned.1.call-update) | async-done | bytes 6291472 | tf_op jit(solution)/shard_map/all_gather | solution.py:23
  237.6 0.0 copy-done.5
  237.6 0.0 copy-done.6
  237.6 12.1 %multiply_convert_fusion = bf16[1024,768]{1,0:T(8,128)(2,1)} fusion(f32[1024,768]{1,0:T(8,128)S(1)} %fusion.8, bf16[1024,4096]{1,0:T(8,128)(2,1)} %all-gather.4.cloned.1.call-done, bf16[4096,768]{1,0:T(8,128)(2,1)} %all-gather.8.cloned.1.call-done, f32[768]{0:T(1024)S(1)} %copy-done.5, f32[768]{0:T(1024)S(1)} %copy-done.6), kind=kOutput, calls=%fused_computation | convolution fusion | flops 6448742400 | bytes 19404800 | tf_op jit(solution)/shard_map/dot_general | solution.py:27
  (2 shorter events, 0.0 us)
Async XLA Ops:
  7.2 3.5 %copy-start.1 = (bf16[128,4096]{1,0:T(8,128)(2,1)S(1)}, bf16[128,4096]{1,0:T(8,128)(2,1)}, u32[]{:S(2)}) copy-start(bf16[128,4096]{1,0:T(8,128)(2,1)} %param.9) | copy-start | bytes 3145732
  7.2 3.8 %copy-start.3 = (f32[4096]{0:T(1024)S(1)}, f32[4096]{0:T(1024)}, u32[]{:S(2)}) copy-start(f32[4096]{0:T(1024)} %param.10) | copy-start | bytes 49156
  7.2 3.8 %copy-start.2 = (bf16[128,4096]{1,0:T(8,128)(2,1)S(1)}, bf16[128,4096]{1,0:T(8,128)(2,1)}, u32[]{:S(2)}) copy-start(bf16[128,4096]{1,0:T(8,128)(2,1)} %param.8) | copy-start | bytes 3145732
  7.2 76.3 %all-gather.6.cloned.1.call-start = ((), (), s32[]{:S(2)}) async-start(), calls=%async_computation.1 | async-start | bytes 7864320 | tf_op jit(solution)/shard_map/all_gather | solution.py:22
  10.6 1.2 copy-start.4
  10.6 156.6 %all-gather.4.cloned.1.call-start = ((), (), s32[]{:S(2)}) async-start(), calls=%async_computation | async-start | bytes 9437184 | tf_op jit(solution)/shard_map/all_gather | solution.py:25
  11.7 4.7 %copy-start = (bf16[128,4096]{1,0:T(8,128)(2,1)}, bf16[128,4096]{1,0:T(8,128)(2,1)S(1)}, u32[]{:S(2)}) copy-start(bf16[128,4096]{1,0:T(8,128)(2,1)S(1)} %get-tuple-element.3) | copy-start | bytes 3145732
  13.1 224.4 %all-gather.8.cloned.1.call-start = ((), (), s32[]{:S(2)}) async-start(), calls=%async_computation.2 | async-start | bytes 7864320 | tf_op jit(solution)/shard_map/all_gather | solution.py:23
  16.4 221.2 %copy-start.5 = (f32[768]{0:T(1024)S(1)}, f32[768]{0:T(1024)}, u32[]{:S(2)}) copy-start(f32[768]{0:T(1024)} %param.15) | copy-start | bytes 9220
  16.4 221.1 %copy-start.6 = (f32[768]{0:T(1024)S(1)}, f32[768]{0:T(1024)}, u32[]{:S(2)}) copy-start(f32[768]{0:T(1024)} %param.14) | copy-start | bytes 9220
Sparse Core Ops, SparseCore 0:
  10.7 72.7 all-gather.5
  85.1 82.0 all-gather.3
  169.0 68.5 all-gather.7
where the time goes:
time: 256 us
  waiting for transfers between devices  210 us (82%)
  matrix products  23 us (9%)
  between operations  13.8 us (5%)
  other arithmetic  8.92 us (3%)
    all_gather x1, waiting for transfers between devices, on_device(): piece = lax.all_gather(normed, 'tp', axis=0, tiled=True)  83.7 us
    all_gather x1, waiting for transfers between devices, on_device(): lax.all_gather(gate_cast, 'fs', axis=0, tiled=True)  67.1 us
    all_gather x1, waiting for transfers between devices, on_device(): lax.all_gather(up_cast, 'fs', axis=0, tiled=True)  59.5 us
    dot_general x1, matrix products, on_device(): up = jnp.dot(piece, up_full, preferred_element_type=jnp.float32) * up_scale  12.1 us
    dot_general x1, matrix products, on_device(): jnp.dot(piece, gate_full, preferred_element_type=jnp.float32) * gate_scale  10.9 us
  transfers between devices with their start and end apart: 3, of which 3 were waited for; matrix products, arithmetic and copies ran while one was open for 6% of the time, Pallas kernels for 0%

commit v1 on v0

--- a/solution.py
+++ b/solution.py
@@ -22,7 +22,9 @@
         lax.all_gather(gate_cast, "fs", axis=0, tiled=True),
         lax.all_gather(up_cast, "fs", axis=0, tiled=True),
     )
-    piece = lax.all_gather(normed, "tp", axis=0, tiled=True)
+    piece = jnp.concatenate(
+        lax.all_to_all(jnp.stack([normed] * lax.axis_size("tp")), "tp", 0, 0), axis=0
+    )
     gate = jnp.dot(piece, gate_full, preferred_element_type=jnp.float32) * gate_scale
     up = jnp.dot(piece, up_full, preferred_element_type=jnp.float32) * up_scale
     hidden = (jax.nn.silu(gate) * up).astype(jnp.bfloat16)

time: 256 us -> 237 us (0.926)
  waiting for transfers between devices: 210 us -> 180 us
  starting transfers between devices: 0.12 us -> 6.43 us
  local copies, waits for them, and re-layouts: 0.04 us -> 4.32 us
    all_to_all x0 -> x1, waiting for transfers between devices: none -> 123 us  [on_device(): lax.all_to_all(jnp.stack([normed] * lax.axis_size('tp')), 'tp', 0, 0)]
    all_gather x1 -> x0, waiting for transfers between devices: 83.7 us -> none  [on_device(): piece = lax.all_gather(normed, 'tp', axis=0, tiled=True)]
    all_gather x1, waiting for transfers between devices: 59.5 us -> 0.02 us  [on_device(): lax.all_gather(up_cast, 'fs', axis=0, tiled=True)]
    all_gather x1, waiting for transfers between devices: 67.1 us -> 57.1 us  [on_device(): lax.all_gather(gate_cast, 'fs', axis=0, tiled=True)]
    all_to_all x0 -> x1, starting transfers between devices: none -> 6.35 us  [on_device(): lax.all_to_all(jnp.stack([normed] * lax.axis_size('tp')), 'tp', 0, 0)]
    another operation x0 -> x1, local copies, waits for them, and re-layouts: none -> 4.29 us  [on_device(): jnp.stack([normed] * lax.axis_size('tp'))]
  transfers between devices with their start and end apart: 3 -> 3, of which waited for: 3 -> 2; matrix products, arithmetic and copies ran while one was open for 6% -> 9% of each run, Pallas kernels for 0% -> 0%
where the time goes in v1:
time: 237 us
  waiting for transfers between devices  180 us (76%)
  matrix products  23 us (10%)
  between operations  14.2 us (6%)
  other arithmetic  8.35 us (4%)
  starting transfers between devices  6.43 us (3%)
  local copies, waits for them, and re-layouts  4.32 us (2%)
    all_to_all x1, waiting for transfers between devices, on_device(): lax.all_to_all(jnp.stack([normed] * lax.axis_size('tp')), 'tp', 0, 0)  123 us
    all_gather x1, waiting for transfers between devices, on_device(): lax.all_gather(gate_cast, 'fs', axis=0, tiled=True)  57.1 us
    dot_general x1, matrix products, on_device(): up = jnp.dot(piece, up_full, preferred_element_type=jnp.float32) * up_scale  12.1 us
    dot_general x1, matrix products, on_device(): jnp.dot(piece, gate_full, preferred_element_type=jnp.float32) * gate_scale  10.9 us
    all_to_all x1, starting transfers between devices, on_device(): lax.all_to_all(jnp.stack([normed] * lax.axis_size('tp')), 'tp', 0, 0)  6.35 us
  transfers between devices with their start and end apart: 3, of which 2 were waited for; matrix products, arithmetic and copies ran while one was open for 9% of the time, Pallas kernels for 0%

profile of v1, /device:TPU:0, one launch (start us, length us, event | category | flops | bytes accessed | tf_op | source)
XLA Modules:
  0.0 236.5 jit_solution(17534407387343520380)
XLA Ops:
  7.2 0.0 copy-start.1
  7.2 0.0 copy-start.3
  7.2 0.0 copy-start.2
  7.2 0.0 all-gather.3.cloned.1.call-start
  7.2 3.3 %convert_element_type.29 = bf16[1024,768]{1,0:T(8,128)(2,1)} convert(f32[1024,768]{1,0:T(8,128)} %param.12) | non-fusion elementwise | flops 786432 | bytes 4718592 | tf_op jit(solution)/shard_map/convert_element_type | solution.py:19
  10.6 0.0 copy-start.4
  10.6 0.0 all-gather.3.cloned.1.call-update
  10.6 0.0 copy-done.1
  10.6 0.3 fusion
  10.9 0.0 copy-done.3
  10.9 0.0 copy-done.2
  10.9 0.7 fusion.4
  11.7 0.0 copy-start
  11.7 0.0 copy-done.4
  11.7 0.3 fusion.6
  12.0 4.3 %stack.2 = bf16[8,128,4096]{2,1,0:T(8,128)(2,1)} broadcast(bf16[128,4096]{1,0:T(8,128)(2,1)S(1)} %fusion.6), dimensions={1,2} | broadcast | bytes 9437184 | tf_op jit(solution)/shard_map/stack | solution.py:26
  16.3 0.0 copy-done
  16.3 6.4 %all-to-all-start = ((bf16[8,128,4096]{2,1,0:T(8,128)(2,1)}), bf16[8,128,4096]{2,1,0:T(8,128)(2,1)}, u32[]{:S(2)}, u32[]{:S(2)}) async-start(bf16[8,128,4096]{2,1,0:T(8,128)(2,1)} %stack.2), calls=%async_computation | async-start | bytes 16777216 | tf_op jit(solution)/shard_map/all_to_all | solution.py:26
  22.7 0.0 all-gather.5.cloned.1.call-start
  22.7 3.7 %convert_element_type.30 = bf16[1024,768]{1,0:T(8,128)(2,1)} convert(f32[1024,768]{1,0:T(8,128)} %param.13) | non-fusion elementwise | flops 786432 | bytes 4718592 | tf_op jit(solution)/shard_map/convert_element_type | solution.py:20
  26.4 0.0 all-gather.5.cloned.1.call-update
  26.4 57.1 %all-gather.3.cloned.1.call-done = bf16[4096,768]{1,0:T(8,128)(2,1)} async-done(((bf16[1024,768]{1,0:T(8,128)(2,1)}), bf16[4096,768]{1,0:T(8,128)(2,1)}) %all-gather.3.cloned.1.call-update) | async-done | bytes 6291472 | tf_op jit(solution)/shard_map/all_gather | solution.py:22
  83.5 123.1 %all-to-all-done = bf16[8,128,4096]{2,1,0:T(8,128)(2,1)} async-done(((bf16[8,128,4096]{2,1,0:T(8,128)(2,1)}), bf16[8,128,4096]{2,1,0:T(8,128)(2,1)}, u32[]{:S(2)}, u32[]{:S(2)}) %all-to-all-start) | async-done | bytes 8388640 | tf_op jit(solution)/shard_map/all_to_all | solution.py:26
  206.6 0.0 copy-start.5
  206.6 0.0 copy-start.6
  206.6 10.9 %fusion.8 = f32[1024,768]{1,0:T(8,128)S(1)} fusion(bf16[1024,4096]{1,0:T(8,128)(2,1)} %bitcast, bf16[4096,768]{1,0:T(8,128)(2,1)} %all-gather.3.cloned.1.call-done), kind=kOutput, calls=%fused_computation.14 | convolution fusion | flops 6442450944 | bytes 17825792 | tf_op jit(solution)/shard_map/dot_general | solution.py:28
  217.6 0.0 all-gather.5.cloned.1.call-done
  217.6 0.0 copy-done.5
  217.6 0.0 copy-done.6
  217.6 12.1 %multiply_convert_fusion = bf16[1024,768]{1,0:T(8,128)(2,1)} fusion(f32[1024,768]{1,0:T(8,128)S(1)} %fusion.8, bf16[1024,4096]{1,0:T(8,128)(2,1)} %bitcast, bf16[4096,768]{1,0:T(8,128)(2,1)} %all-gather.5.cloned.1.call-done, f32[768]{0:T(1024)S(1)} %copy-done.5, f32[768]{0:T(1024)S(1)} %copy-done.6), kind=kOutput, calls=%fused_computation | convolution fusion | flops 6448742400 | bytes 19404800 | tf_op jit(solution)/shard_map/dot_general | solution.py:29
  (2 shorter events, 0.0 us)
Async XLA Ops:
  7.2 3.4 %copy-start.1 = (bf16[128,4096]{1,0:T(8,128)(2,1)S(1)}, bf16[128,4096]{1,0:T(8,128)(2,1)}, u32[]{:S(2)}) copy-start(bf16[128,4096]{1,0:T(8,128)(2,1)} %param.9) | copy-start | bytes 3145732
  7.2 3.7 %copy-start.3 = (f32[4096]{0:T(1024)S(1)}, f32[4096]{0:T(1024)}, u32[]{:S(2)}) copy-start(f32[4096]{0:T(1024)} %param.10) | copy-start | bytes 49156
  7.2 3.7 %copy-start.2 = (bf16[128,4096]{1,0:T(8,128)(2,1)S(1)}, bf16[128,4096]{1,0:T(8,128)(2,1)}, u32[]{:S(2)}) copy-start(bf16[128,4096]{1,0:T(8,128)(2,1)} %param.8) | copy-start | bytes 3145732
  7.2 76.3 %all-gather.3.cloned.1.call-start = ((), (), s32[]{:S(2)}) async-start(), calls=%async_computation.1 | async-start | bytes 7864320 | tf_op jit(solution)/shard_map/all_gather | solution.py:22
  10.6 1.1 copy-start.4
  11.7 4.7 %copy-start = (bf16[128,4096]{1,0:T(8,128)(2,1)}, bf16[128,4096]{1,0:T(8,128)(2,1)S(1)}, u32[]{:S(2)}) copy-start(bf16[128,4096]{1,0:T(8,128)(2,1)S(1)} %get-tuple-element.3) | copy-start | bytes 3145732
  16.3 190.3 %all-to-all-start = ((bf16[8,128,4096]{2,1,0:T(8,128)(2,1)}), bf16[8,128,4096]{2,1,0:T(8,128)(2,1)}, u32[]{:S(2)}, u32[]{:S(2)}) async-start(bf16[8,128,4096]{2,1,0:T(8,128)(2,1)} %stack.2), calls=%async_computation | async-start | bytes 16777216 | tf_op jit(solution)/shard_map/all_to_all | solution.py:26
  22.7 194.9 %all-gather.5.cloned.1.call-start = ((), (), s32[]{:S(2)}) async-start(), calls=%async_computation.2 | async-start | bytes 7864320 | tf_op jit(solution)/shard_map/all_gather | solution.py:23
  206.6 11.0 %copy-start.5 = (f32[768]{0:T(1024)S(1)}, f32[768]{0:T(1024)}, u32[]{:S(2)}) copy-start(f32[768]{0:T(1024)} %param.15) | copy-start | bytes 9220
  206.6 11.0 %copy-start.6 = (f32[768]{0:T(1024)S(1)}, f32[768]{0:T(1024)}, u32[]{:S(2)}) copy-start(f32[768]{0:T(1024)} %param.14) | copy-start | bytes 9220
Sparse Core Ops, SparseCore 0:
  10.7 72.7 all-gather.2
  85.3 70.0 all-gather.4
